TPU v7x, 32 devices: a whole 2x2x4 slice. The times are simulated.
32 devices in a mesh: ep: 8 (over z, x), tp: 4 (over y, core).
Axes of the slice: x: 2, y: 2, z: 4, core: 2. Of those that a mesh axis runs over, the one named last changes fastest.
Arguments:
- projected_queries: bfloat16 [2048, 2048], P('ep', 'tp'), may hold values from -245 to 245, as said below
- key_proj: bfloat16 [2048, 512], P('ep', 'tp'), may hold values from -6.2 to 6.2
- projected_values: bfloat16 [2048, 512], P('ep', 'tp'), may hold values from -24 to 24
- head_sink_logits: float32 [32], P('tp'), may hold values from 1 to 6
- out_weight: bfloat16 [2048, 4096], P('tp'), may hold values from -0.125 to 0.125
- expert_input: bfloat16 [1024, 4096], P('ep'), may hold values from -6 to 6
- norm_gain: float32 [4096], replicated, may hold values from 0.1 to 1.9
- routing: int32 [1024, 4], P('ep'), may hold values from 0 to 7, all different within a row; in each aligned block of 128 rows (0 to 127, 128 to 255, ...) at most 96 rows name the same one
- route_weight: float32 [1024, 4], P('ep'), may hold values from 0.1 to 1
- gate_weight: bfloat16 [8, 4096, 1024], P('ep', None, 'tp'), may hold values from -0.27929688 to 0.27929688
- up_weight: bfloat16 [8, 4096, 1024], P('ep', None, 'tp'), may hold values from -0.27929688 to 0.27929688
- down_weight: bfloat16 [8, 1024, 4096], P('ep', 'tp'), may hold values from -0.046875 to 0.046875
Outputs:
- mixer_output: bfloat16 [2048, 4096], P(('ep', 'tp'))
- expert_output: bfloat16 [1024, 4096], P('ep', 'tp')
Inputs may be any that keep to these rules, and one draw needn't show every extreme that they name: `projected_queries`: in the hidden draw some queries nearly equal a large multiple of a nearby key. `routing`: each row names 4 different experts; among the rows of one device (aligned blocks of 128 rows) no expert is named more than 96 times, a bound that some block reaches.
All inputs are finite; a program needn't handle non-finite values.
Results may differ from a plain program's by a relative error of at most 0.014.
Values may be sent and summed in bfloat16 or wider, within the bound.
A program may use at most 128 MiB of HBM per device.

v0:
```python
import jax
import jax.numpy as jnp
from jax import lax
from jax.sharding import PartitionSpec as P

D = 4096
HEAD_SIZE = 64
WINDOW_KEYS = 128
TOPK = 4
EPS = 1e-06
CLAMP = 7.0
SLOPE = 1.702


def passed_along(block, axis, distance):
    devices = range(lax.axis_size(axis))
    route = [(i - distance, i) for i in devices if i - distance in devices]
    return lax.ppermute(block, axis, route)


def shards(
    projected_queries,
    key_proj,
    projected_values,
    head_sink_logits,
    out_weight,
    expert_input,
    norm_gain,
    routing,
    route_weight,
    gate_weight,
    up_weight,
    down_weight,
):
    query_rows = projected_queries.shape[0]
    kv_heads = key_proj.shape[1] // HEAD_SIZE
    heads_per_group = projected_queries.shape[1] // HEAD_SIZE // kv_heads
    count_of_blocks = query_rows // WINDOW_KEYS
    prior_key, prior_value = passed_along(
        (key_proj[query_rows - WINDOW_KEYS :], projected_values[query_rows - WINDOW_KEYS :]),
        "ep",
        1,
    )
    key_all = jnp.concatenate([prior_key, key_proj], axis=0)
    value_all = jnp.concatenate([prior_value, projected_values], axis=0)
    window_keys = jnp.concatenate(
        [
            key_all[:-WINDOW_KEYS].reshape(count_of_blocks, WINDOW_KEYS, kv_heads, HEAD_SIZE),
            key_all[WINDOW_KEYS:].reshape(count_of_blocks, WINDOW_KEYS, kv_heads, HEAD_SIZE),
        ],
        axis=1,
    )
    window_values = jnp.concatenate(
        [
            value_all[:-WINDOW_KEYS].reshape(count_of_blocks, WINDOW_KEYS, kv_heads, HEAD_SIZE),
            value_all[WINDOW_KEYS:].reshape(count_of_blocks, WINDOW_KEYS, kv_heads, HEAD_SIZE),
        ],
        axis=1,
    )
    query_blocks = projected_queries.reshape(
        count_of_blocks, WINDOW_KEYS, kv_heads, heads_per_group, HEAD_SIZE
    )
    scores = jnp.einsum(
        "nqhgd,nshd->nhgqs", query_blocks, window_keys, preferred_element_type=jnp.float32
    ) * HEAD_SIZE ** (-0.5)
    offset = lax.axis_index("ep") * query_rows
    block_ids = jnp.arange(count_of_blocks)[:, None, None] * WINDOW_KEYS + offset
    query_pos = block_ids + jnp.arange(WINDOW_KEYS)[None, :, None]
    key_pos = block_ids - WINDOW_KEYS + jnp.arange(2 * WINDOW_KEYS)[None, None, :]
    permitted_mask = (key_pos <= query_pos) & (query_pos - key_pos < WINDOW_KEYS) & (key_pos >= 0)
    scores = jnp.where(permitted_mask[:, None, None, :, :], scores, -jnp.inf)
    sink_col = head_sink_logits.reshape(kv_heads, heads_per_group)[None, :, :, None, None]
    highest = jnp.maximum(jnp.max(scores, axis=-1, keepdims=True), sink_col)
    numerator = jnp.exp(scores - highest)
    denominator = jnp.sum(numerator, axis=-1, keepdims=True) + jnp.exp(sink_col - highest)
    weights = (numerator / denominator).astype(jnp.bfloat16)
    attended = jnp.einsum(
        "nhgqs,nshd->nqhgd", weights, window_values, preferred_element_type=jnp.float32
    )
    attended = attended.astype(jnp.bfloat16).reshape(
        query_rows, kv_heads * heads_per_group * HEAD_SIZE
    )
    mixer_output = lax.psum_scatter(
        jnp.dot(attended, out_weight, preferred_element_type=jnp.float32).astype(jnp.bfloat16),
        "tp",
        scatter_dimension=0,
        tiled=True,
    )
    token_rows = expert_input.shape[0]
    experts = lax.axis_size("ep")
    capacity = max(3 * token_rows * TOPK // (2 * experts), 2)
    col_share = D // lax.axis_size("tp")
    widened = expert_input.astype(jnp.float32)
    normed = (
        widened
        * lax.rsqrt(jnp.mean(widened * widened, axis=-1, keepdims=True) + EPS)
        * norm_gain[None, :]
    ).astype(jnp.bfloat16)
    flat_ids = routing.reshape(-1)
    onehot = (flat_ids[:, None] == jnp.arange(experts, dtype=jnp.int32)[None, :]).astype(jnp.int32)
    rank_in = jnp.cumsum(onehot, axis=0) - 1
    target = flat_ids * capacity + jnp.sum(rank_in * onehot, axis=1)
    tok_ids = jnp.arange(token_rows * TOPK) // TOPK
    slot_tok = jnp.full((experts * capacity,), token_rows, jnp.int32).at[target].set(tok_ids)
    gate_one = gate_weight[0]
    up_one = up_weight[0]
    own_cols = lax.dynamic_slice_in_dim(normed, lax.axis_index("tp") * col_share, col_share, 1)
    extended = jnp.concatenate([own_cols, jnp.zeros((1, col_share), jnp.bfloat16)], axis=0)
    outgoing = jnp.take(extended, slot_tok, axis=0).reshape(experts, capacity, col_share)
    arrived = lax.all_to_all(outgoing, "ep", split_axis=0, concat_axis=0, tiled=True).reshape(
        experts * capacity, col_share
    )
    portion = lax.all_gather(arrived, "tp", axis=1, tiled=True)
    gate_pre = jnp.dot(portion, gate_one, preferred_element_type=jnp.float32)
    up_pre = jnp.dot(portion, up_one, preferred_element_type=jnp.float32)
    gate_cut = jnp.minimum(gate_pre, CLAMP)
    activated = (
        (jnp.clip(up_pre, -CLAMP, CLAMP) + 1.0) * gate_cut * jax.nn.sigmoid(SLOPE * gate_cut)
    ).astype(jnp.bfloat16)
    partial_value = jnp.dot(activated, down_weight[0], preferred_element_type=jnp.float32)
    expert_result = lax.psum_scatter(
        partial_value.astype(jnp.bfloat16), "tp", scatter_dimension=1, tiled=True
    )
    returned = lax.all_to_all(
        expert_result.reshape(experts, capacity, col_share),
        "ep",
        split_axis=0,
        concat_axis=0,
        tiled=True,
    )
    picked = jnp.take(returned.reshape(experts * capacity, col_share), target, axis=0)
    picked = picked.astype(jnp.float32).reshape(token_rows, TOPK, col_share)
    expert_output = jnp.sum(picked * route_weight[:, :, None], axis=1).astype(jnp.bfloat16)
    return (mixer_output, expert_output)


def solution(mesh):
    placed = (
        P("ep", "tp"),
        P("ep", "tp"),
        P("ep", "tp"),
        P("tp"),
        P("tp", None),
        P("ep", None),
        P(),
        P("ep", None),
        P("ep", None),
        P("ep", None, "tp"),
        P("ep", None, "tp"),
        P("ep", "tp", None),
    )
    return jax.shard_map(
        shards,
        mesh=mesh,
        in_specs=placed,
        out_specs=(P(("ep", "tp"), None), P("ep", "tp")),
        check_vma=False,
    )
```

profile of v0, /device:TPU:0, one launch (start us, length us, event | category | flops | bytes accessed | tf_op | source)
XLA Modules:
  0.0 246.2 jit_solution(7340603953749888694)
XLA Ops:
  7.2 2.9 %convert_element_type.41 = f32[128,4096]{1,0:T(8,128)} convert(bf16[128,4096]{1,0:T(8,128)(2,1)} %param.17) | non-fusion elementwise | flops 524288 | bytes 3145728 | tf_op jit(solution)/shard_map/convert_element_type | solution.py:93
  10.2 0.3 multiply_reduce_fusion.1
  10.8 1.1 reduce-window.6
  12.0 0.2 slice_reduce_fusion
  12.6 2.4 scatter_custom_fusion
  15.2 0.7 dynamic-slice
  15.9 1.1 fusion.33
  17.1 3.6 %gather_fusion = bf16[768,1024]{1,0:T(8,128)(2,1)} fusion(bf16[129,1024]{1,0:T(8,128)(2,1)S(1)} %concatenate.19, s32[1024]{0:T(1024)S(1)} %pad_clamp_fusion.1), kind=kCustom, calls=%fused_computation | custom fusion | bytes 3148800 | tf_op jit(solution)/shard_map/jit(_take)/gather | solution.py:109
  20.6 1.6 broadcast_select_fusion
  22.3 44.2 %all_to_all.10 = bf16[8,96,1024]{2,1,0:T(8,128)(2,1)} all-to-all(bf16[8,96,1024]{2,1,0:T(8,128)(2,1)S(1)} %broadcast_select_fusion), channel_id=1, replica_groups=mesh['ep'=8,'tp'=4] {'ep'}, dimensions={0} | all-to-all | bytes 3145728 | tf_op jit(solution)/shard_map/all_to_all | solution.py:110
  66.5 45.5 %all-gather.2.cloned.1.call-done = bf16[768,4096]{1,0:T(8,128)(2,1)} async-done(((bf16[768,1024]{1,0:T(8,128)(2,1)}), bf16[768,4096]{1,0:T(8,128)(2,1)}) %all-gather.2.cloned.1.call-update) | async-done | bytes 6291472 | tf_op jit(solution)/shard_map/all_gather | solution.py:113
  112.0 5.2 %fusion.9 = f32[768,256]{1,0:T(8,128)S(1)} fusion(bf16[768,4096]{1,0:T(8,128)(2,1)} %all-gather.2.cloned.1.call-done, bf16[1,4096,256]{2,1,0:T(8,128)(2,1)} %param.21), kind=kOutput, calls=%fused_computation.18 | convolution fusion | flops 1610809344 | bytes 9175040 | tf_op jit(solution)/shard_map/dot_general | solution.py:114
  117.2 12.7 %convolution_convert_fusion = bf16[768,4096]{1,0:T(8,128)(2,1)} fusion(bf16[1,256,4096]{2,1,0:T(8,128)(2,1)S(1)} %copy-done, f32[768,256]{1,0:T(8,128)S(1)} %fusion.9, bf16[768,4096]{1,0:T(8,128)(2,1)} %all-gather.2.cloned.1.call-done, bf16[1,4096,256]{2,1,0:T(8,128)(2,1)} %param.22), kind=kOutput, calls=%fused_computation.3 | convolution fusion | flops 3226140672 | bytes 17563648 | tf_op jit(solution)/shard_map/dot_general | solution.py:120
  130.0 0.8 copy-done.3
  130.8 3.4 %collective-permute-start.1 = (bf16[128,128]{1,0:T(8,128)(2,1)S(1)}, bf16[128,128]{1,0:T(8,128)(2,1)S(1)}, u32[]{:S(2)}, u32[]{:S(2)}) collective-permute-start(bf16[128,128]{1,0:T(8,128)(2,1)S(1)} %slice.20), channel_id=1, source_target_pairs={{0,4},{4,8},{8,12},{12,16},{16,20},{20,24},{24,28},{1,5},{5,9},{9,... | collective-permute-start | bytes 98312 | tf_op jit(solution)/shard_map/ppermute | solution.py:18
  134.2 3.6 %collective-permute-start = (bf16[128,128]{1,0:T(8,128)(2,1)S(1)}, bf16[128,128]{1,0:T(8,128)(2,1)S(1)}, u32[]{:S(2)}, u32[]{:S(2)}) collective-permute-start(bf16[128,128]{1,0:T(8,128)(2,1)S(1)} %slice.18), channel_id=1, source_target_pairs={{0,4},{4,8},{8,12},{12,16},{16,20},{20,24},{24,28},{1,5},{5,9},{9,... | collective-permute-start | bytes 98312 | tf_op jit(solution)/shard_map/ppermute | solution.py:18
  138.0 0.2 fusion.42
  138.4 0.3 reshape.255
  139.5 0.5 fusion.60
  140.1 0.3 fusion.5
  140.5 0.5 fusion.26
  141.0 0.3 copy.45
  141.2 1.7 copy-done.2
  143.0 2.7 %convolution_convert_fusion.1 = bf16[256,4096]{1,0:T(8,128)(2,1)} fusion(bf16[512,4096]{1,0:T(8,128)(2,1)S(1)} %copy-done.2, bf16[64,8,2,128]{3,2,1,0:T(2,128)(2,1)S(1)} %bitcast.64), kind=kOutput, calls=%fused_computation.4 | convolution fusion | flops 1074790400 | bytes 6553600 | tf_op jit(solution)/shard_map/dot_general | solution.py:84
  145.7 42.3 %reduce-scatter.5.cloned.1.call-done = bf16[768,1024]{1,0:T(8,128)(2,1)} async-done(((bf16[768,4096]{1,0:T(8,128)(2,1)}), bf16[768,1024]{1,0:T(8,128)(2,1)}) %reduce-scatter.5.cloned.1.call-update) | async-done | bytes 1572880 | tf_op jit(solution)/shard_map/reduce_scatter | solution.py:121
  188.0 5.5 %all-to-all-start.1 = ((bf16[8,96,1024]{2,1,0:T(8,128)(2,1)}), bf16[8,96,1024]{2,1,0:T(8,128)(2,1)}, u32[]{:S(2)}, u32[]{:S(2)}) async-start(bf16[8,96,1024]{2,1,0:T(8,128)(2,1)} %bitcast.63), calls=%async_computation.3 | async-start | bytes 3145728 | tf_op jit(solution)/shard_map/all_to_all | solution.py:124
  193.7 0.1 copy.49
  193.9 0.1 copy.51
  194.0 36.5 %all-to-all-done.1 = bf16[8,96,1024]{2,1,0:T(8,128)(2,1)} async-done(((bf16[8,96,1024]{2,1,0:T(8,128)(2,1)}), bf16[8,96,1024]{2,1,0:T(8,128)(2,1)}, u32[]{:S(2)}, u32[]{:S(2)}) %all-to-all-start.1) | async-done | bytes 1572896 | tf_op jit(solution)/shard_map/all_to_all | solution.py:124
  230.4 4.3 %gather_fusion.1 = bf16[512,1024]{1,0:T(8,128)(2,1)S(1)} fusion(bf16[768,1024]{1,0:T(8,128)(2,1)} %bitcast.16, s32[1024]{0:T(1024)S(1)} %pad_clamp_fusion), kind=kCustom, calls=%fused_computation.1 | custom fusion | bytes 2099200 | tf_op jit(solution)/shard_map/jit(_take)/gather | solution.py:131
  234.8 1.2 gather.15
  236.0 3.6 %multiply_reduce_fusion = bf16[128,1024]{1,0:T(8,128)(2,1)} fusion(f32[128,4]{1,0:T(8,128)S(1)} %copy.51, bf16[128,4,1024]{2,1,0:T(4,128)(2,1)} %gather.15, pred[128,4]{1,0:T(8,128)(4,1)S(1)} %copy.49), kind=kLoop, calls=%fused_computation.11 | loop fusion | flops 1966080 | bytes 1313280 | tf_op jit(solution)/shard_map/reduce_sum | solution.py:133
  (66 shorter events, 2.5 us)
Async XLA Ops:
  7.2 110.1 %copy-start = (bf16[1,256,4096]{2,1,0:T(8,128)(2,1)S(1)}, bf16[1,256,4096]{2,1,0:T(8,128)(2,1)}, u32[]{:S(2)}) copy-start(bf16[1,256,4096]{2,1,0:T(8,128)(2,1)} %param.23) | copy-start | bytes 6291460
  7.2 3.0 %copy-start.1 = (bf16[128,4096]{1,0:T(8,128)(2,1)S(1)}, bf16[128,4096]{1,0:T(8,128)(2,1)}, u32[]{:S(2)}) copy-start(bf16[128,4096]{1,0:T(8,128)(2,1)} %param.17) | copy-start | bytes 3145732
  7.2 104.8 %all-gather.2.cloned.1.call-start = ((), (), s32[]{:S(2)}) async-start(), calls=%async_computation.5 | async-start | bytes 7864320 | tf_op jit(solution)/shard_map/all_gather | solution.py:113
  7.2 3.2 %copy-start.6 = (s32[128,4]{0,1:T(4,128)S(1)}, s32[128,4]{0,1:T(4,128)}, u32[]{:S(2)}) copy-start(s32[128,4]{0,1:T(4,128)} %param.19) | copy-start | bytes 6148
  66.5 121.5 %reduce-scatter.5.cloned.1.call-start = ((), (), s32[]{:S(2)}) async-start(), calls=%async_computation.6 | async-start | bytes 7864320 | tf_op jit(solution)/shard_map/reduce_scatter | solution.py:121
  129.9 0.8 copy-start.3
  129.9 4.2 %copy-start.4 = (bf16[256,128]{1,0:T(8,128)(2,1)S(1)}, bf16[256,128]{1,0:T(8,128)(2,1)}, u32[]{:S(2)}) copy-start(bf16[256,128]{1,0:T(8,128)(2,1)} %param.14) | copy-start | bytes 196612
  129.9 8.5 %copy-start.5 = (bf16[256,512]{1,0:T(8,128)(2,1)S(1)}, bf16[256,512]{1,0:T(8,128)(2,1)}, u32[]{:S(2)}) copy-start(bf16[256,512]{1,0:T(8,128)(2,1)} %param.12) | copy-start | bytes 786436
  129.9 8.9 %copy-start.8 = (f32[8]{0:T(128)S(1)}, f32[8]{0:T(128)}, u32[]{:S(2)}) copy-start(f32[8]{0:T(128)} %param.15) | copy-start | bytes 100
  130.0 109.7 %reduce-scatter.3.cloned.1.call-start = ((), (), s32[]{:S(2)}) async-start(), calls=%async_computation.4 | async-start | bytes 2621440 | tf_op jit(solution)/shard_map/reduce_scatter | solution.py:83
  130.8 8.2 %collective-permute-start.1 = (bf16[128,128]{1,0:T(8,128)(2,1)S(1)}, bf16[128,128]{1,0:T(8,128)(2,1)S(1)}, u32[]{:S(2)}, u32[]{:S(2)}) collective-permute-start(bf16[128,128]{1,0:T(8,128)(2,1)S(1)} %slice.20), channel_id=1, source_target_pairs={{0,4},{4,8},{8,12},{12,16},{16,20},{20,24},{24,28},{1,5},{5,9},{9,... | collective-permute-start | bytes 98312 | tf_op jit(solution)/shard_map/ppermute | solution.py:18
  134.2 5.1 %collective-permute-start = (bf16[128,128]{1,0:T(8,128)(2,1)S(1)}, bf16[128,128]{1,0:T(8,128)(2,1)S(1)}, u32[]{:S(2)}, u32[]{:S(2)}) collective-permute-start(bf16[128,128]{1,0:T(8,128)(2,1)S(1)} %slice.18), channel_id=1, source_target_pairs={{0,4},{4,8},{8,12},{12,16},{16,20},{20,24},{24,28},{1,5},{5,9},{9,... | collective-permute-start | bytes 98312 | tf_op jit(solution)/shard_map/ppermute | solution.py:18
  140.5 2.5 %copy-start.2 = (bf16[512,4096]{1,0:T(8,128)(2,1)S(1)}, bf16[512,4096]{1,0:T(8,128)(2,1)}, u32[]{:S(2)}) copy-start(bf16[512,4096]{1,0:T(8,128)(2,1)} %param.16) | copy-start | bytes 12582916
  145.7 48.2 %copy-start.7 = (f32[128,4]{0,1:T(4,128)S(1)}, f32[128,4]{0,1:T(4,128)}, u32[]{:S(2)}) copy-start(f32[128,4]{0,1:T(4,128)} %param.20) | copy-start | bytes 6148
  188.0 42.4 %all-to-all-start.1 = ((bf16[8,96,1024]{2,1,0:T(8,128)(2,1)}), bf16[8,96,1024]{2,1,0:T(8,128)(2,1)}, u32[]{:S(2)}, u32[]{:S(2)}) async-start(bf16[8,96,1024]{2,1,0:T(8,128)(2,1)} %bitcast.63), calls=%async_computation.3 | async-start | bytes 3145728 | tf_op jit(solution)/shard_map/all_to_all | solution.py:124
Sparse Core Ops, SparseCore 0:
  66.6 45.3 all-gather.1
  130.1 57.8 reduce-scatter.4
  191.1 31.1 reduce-scatter.2
where the time goes:
time: 247 us; the launch traced here: 246 us
  waiting for transfers between devices  124 us (50%)
  blocking collectives  44.2 us (18%)
  matrix products  21.6 us (9%)
  local copies, waits for them, and re-layouts  17.5 us (7%)
  between operations  14.1 us (6%)
  starting transfers between devices  12.6 us (5%)
  other arithmetic  11.9 us (5%)
    all_gather x1, waiting for transfers between devices, shards(): portion = lax.all_gather(arrived, 'tp', axis=1, tiled=True)  45.5 us
    all_to_all x1, blocking collectives, shards(): lax.all_to_all(outgoing, 'ep', split_axis=0, concat_axis=0, tiled=True)  44.2 us
    reduce_scatter x1, waiting for transfers between devices, shards(): lax.psum_scatter(partial_value.astype(jnp.bfloat16), 'tp', scatter_dimens...  42.3 us
    all_to_all x1, waiting for transfers between devices, shards(): lax.all_to_all(expert_result.reshape(experts, capacity, col_share), 'ep',...  36.5 us
    dot_general x1, matrix products, shards(): jnp.dot(activated, down_weight[0], preferred_element_type=jnp.float32)  12.7 us
    ppermute x2, starting transfers between devices, passed_along(): return lax.ppermute(block, axis, route)  6.93 us
    gather x2, local copies, waits for them, and re-layouts, shards(): jnp.take(returned.reshape(experts * capacity, col_share), target, axis=0)  5.57 us
    all_to_all x1, starting transfers between devices, shards(): lax.all_to_all(expert_result.reshape(experts, capacity, col_share), 'ep',...  5.51 us
  transfers between devices with their start and end apart: 6, of which 3 were waited for; matrix products, arithmetic and copies ran while one was open for 6% of the time, Pallas kernels for 0%

commit v1 on v0

--- a/solution.py
+++ b/solution.py
@@ -110,7 +110,9 @@
     arrived = lax.all_to_all(outgoing, "ep", split_axis=0, concat_axis=0, tiled=True).reshape(
         experts * capacity, col_share
     )
-    portion = lax.all_gather(arrived, "tp", axis=1, tiled=True)
+    portion = jnp.concatenate(
+        lax.all_to_all(jnp.stack([arrived] * lax.axis_size("tp")), "tp", 0, 0), axis=1
+    )
     gate_pre = jnp.dot(portion, gate_one, preferred_element_type=jnp.float32)
     up_pre = jnp.dot(portion, up_one, preferred_element_type=jnp.float32)
     gate_cut = jnp.minimum(gate_pre, CLAMP)

time: 247 us -> 277 us (1.12)
  blocking collectives: 44.2 us -> 118 us
  waiting for transfers between devices: 124 us -> 77.4 us
  local copies, waits for them, and re-layouts: 17.5 us -> 24.5 us
  matrix products: 21.6 us -> 18.2 us
    all_to_all x0 -> x1, blocking collectives: none -> 73.4 us  [shards(): lax.all_to_all(jnp.stack([arrived] * lax.axis_size('tp')), 'tp', 0, 0)]
    all_gather x1 -> x0, waiting for transfers between devices: 45.5 us -> none  [shards(): portion = lax.all_gather(arrived, 'tp', axis=1, tiled=True)]
    another operation x1 -> x3, local copies, waits for them, and re-layouts: 0.01 us -> 4.41 us  [the longest x2 4.4 us: shards(): jnp.stack([arrived] * lax.axis_size('tp'))]
    dot_general x1, matrix products: 5.2 us -> 1.82 us  [shards(): gate_pre = jnp.dot(portion, gate_one, preferred_element_type=jnp.float32)]
  transfers between devices with their start and end apart: 6 -> 5, of which waited for: 3 -> 2; matrix products, arithmetic and copies ran while one was open for 6% -> 6% of each run, Pallas kernels for 0% -> 0%
where the time goes in v1:
time: 277 us; the launch traced here: 276 us
  blocking collectives  118 us (43%)
  waiting for transfers between devices  77.4 us (28%)
  local copies, waits for them, and re-layouts  24.5 us (9%)
  matrix products  18.2 us (7%)
  between operations  14.4 us (5%)
  starting transfers between devices  12.1 us (4%)
  other arithmetic  11.9 us (4%)
    all_to_all x1, blocking collectives, shards(): lax.all_to_all(jnp.stack([arrived] * lax.axis_size('tp')), 'tp', 0, 0)  73.4 us
    all_to_all x1, blocking collectives, shards(): lax.all_to_all(outgoing, 'ep', split_axis=0, concat_axis=0, tiled=True)  44.2 us
    reduce_scatter x1, waiting for transfers between devices, shards(): lax.psum_scatter(partial_value.astype(jnp.bfloat16), 'tp', scatter_dimens...  40.9 us
    all_to_all x1, waiting for transfers between devices, shards(): lax.all_to_all(expert_result.reshape(experts, capacity, col_share), 'ep',...  36.5 us
    dot_general x1, matrix products, shards(): jnp.dot(activated, down_weight[0], preferred_element_type=jnp.float32)  12.7 us
    ppermute x2, starting transfers between devices, passed_along(): return lax.ppermute(block, axis, route)  6.51 us
    gather x2, local copies, waits for them, and re-layouts, shards(): jnp.take(returned.reshape(experts * capacity, col_share), target, axis=0)  5.57 us
  transfers between devices with their start and end apart: 5, of which 2 were waited for; matrix products, arithmetic and copies ran while one was open for 6% of the time, Pallas kernels for 0%

profile of v1, /device:TPU:0, one launch (start us, length us, event | category | flops | bytes accessed | tf_op | source)
XLA Modules:
  0.0 276.1 jit_solution(7691838810430235147)
XLA Ops:
  7.2 2.9 %convert_element_type.41 = f32[128,4096]{1,0:T(8,128)} convert(bf16[128,4096]{1,0:T(8,128)(2,1)} %param.17) | non-fusion elementwise | flops 524288 | bytes 3145728 | tf_op jit(solution)/shard_map/convert_element_type | solution.py:93
  10.2 0.3 multiply_reduce_fusion.1
  10.8 1.1 reduce-window.6
  12.0 0.2 slice_reduce_fusion
  12.6 2.4 scatter_custom_fusion
  15.2 0.7 dynamic-slice
  15.9 1.1 fusion.33
  17.1 3.6 %gather_fusion = bf16[768,1024]{1,0:T(8,128)(2,1)} fusion(bf16[129,1024]{1,0:T(8,128)(2,1)S(1)} %concatenate.19, s32[1024]{0:T(1024)S(1)} %pad_clamp_fusion.1), kind=kCustom, calls=%fused_computation | custom fusion | bytes 3148800 | tf_op jit(solution)/shard_map/jit(_take)/gather | solution.py:109
  20.6 1.6 broadcast_select_fusion
  22.3 44.2 %all_to_all.15 = bf16[8,96,1024]{2,1,0:T(8,128)(2,1)} all-to-all(bf16[8,96,1024]{2,1,0:T(8,128)(2,1)S(1)} %broadcast_select_fusion), channel_id=1, replica_groups=mesh['ep'=8,'tp'=4] {'ep'}, dimensions={0} | all-to-all | bytes 3145728 | tf_op jit(solution)/shard_map/all_to_all | solution.py:110
  66.4 2.6 copy.52
  69.0 1.8 stack.3
  70.9 73.4 %all_to_all.16 = bf16[4,768,1024]{1,2,0:T(8,128)(2,1)S(1)} all-to-all(bf16[4,768,1024]{1,2,0:T(8,128)(2,1)S(1)} %stack.3), channel_id=1, replica_groups=mesh['ep'=8,'tp'=4] {'tp'}, dimensions={0} | all-to-all | bytes 12582912 | tf_op jit(solution)/shard_map/all_to_all | solution.py:114
  144.3 2.7 copy-done.1
  146.9 1.8 fusion.9
  148.8 12.7 %convolution_convert_fusion = bf16[768,4096]{1,0:T(8,128)(2,1)} fusion(bf16[1,256,4096]{2,1,0:T(8,128)(2,1)S(1)} %copy-done, f32[768,256]{1,0:T(8,128)S(1)} %fusion.9, bf16[768,4096]{0,1:T(8,128)(2,1)} %bitcast.65, bf16[1,4096,256]{2,1,0:T(8,128)(2,1)} %param.22), kind=kOutput, calls=%fused_computation.3 | convolution fusion | flops 3226140672 | bytes 17563648 | tf_op jit(solution)/shard_map/dot_general | solution.py:122
  161.5 0.8 copy-done.5
  162.3 3.3 %collective-permute-start.1 = (bf16[128,128]{1,0:T(8,128)(2,1)S(1)}, bf16[128,128]{1,0:T(8,128)(2,1)S(1)}, u32[]{:S(2)}, u32[]{:S(2)}) collective-permute-start(bf16[128,128]{1,0:T(8,128)(2,1)S(1)} %slice.20), channel_id=1, source_target_pairs={{0,4},{4,8},{8,12},{12,16},{16,20},{20,24},{24,28},{1,5},{5,9},{9,... | collective-permute-start | bytes 98312 | tf_op jit(solution)/shard_map/ppermute | solution.py:18
  165.6 3.2 %collective-permute-start = (bf16[128,128]{1,0:T(8,128)(2,1)S(1)}, bf16[128,128]{1,0:T(8,128)(2,1)S(1)}, u32[]{:S(2)}, u32[]{:S(2)}) collective-permute-start(bf16[128,128]{1,0:T(8,128)(2,1)S(1)} %slice.18), channel_id=1, source_target_pairs={{0,4},{4,8},{8,12},{12,16},{16,20},{20,24},{24,28},{1,5},{5,9},{9,... | collective-permute-start | bytes 98312 | tf_op jit(solution)/shard_map/ppermute | solution.py:18
  169.5 0.3 reshape.261
  170.6 0.5 fusion.60
  171.2 0.3 fusion.5
  171.6 0.5 fusion.26
  172.1 0.3 copy.46
  172.4 1.6 copy-done.3
  174.0 2.7 convolution_convert_fusion.1
  176.7 40.9 %reduce-scatter.5.cloned.1.call-done = bf16[768,1024]{1,0:T(8,128)(2,1)} async-done(((bf16[768,4096]{1,0:T(8,128)(2,1)}), bf16[768,1024]{1,0:T(8,128)(2,1)}) %reduce-scatter.5.cloned.1.call-update) | async-done | bytes 1572880 | tf_op jit(solution)/shard_map/reduce_scatter | solution.py:123
  217.6 5.5 %all-to-all-start.2 = ((bf16[8,96,1024]{2,1,0:T(8,128)(2,1)}), bf16[8,96,1024]{2,1,0:T(8,128)(2,1)}, u32[]{:S(2)}, u32[]{:S(2)}) async-start(bf16[8,96,1024]{2,1,0:T(8,128)(2,1)} %bitcast.68), calls=%async_computation.4 | async-start | bytes 3145728 | tf_op jit(solution)/shard_map/all_to_all | solution.py:126
  223.6 36.5 %all-to-all-done.2 = bf16[8,96,1024]{2,1,0:T(8,128)(2,1)} async-done(((bf16[8,96,1024]{2,1,0:T(8,128)(2,1)}), bf16[8,96,1024]{2,1,0:T(8,128)(2,1)}, u32[]{:S(2)}, u32[]{:S(2)}) %all-to-all-start.2) | async-done | bytes 1572896 | tf_op jit(solution)/shard_map/all_to_all | solution.py:126
  260.1 4.3 %gather_fusion.1 = bf16[512,1024]{1,0:T(8,128)(2,1)S(1)} fusion(bf16[768,1024]{1,0:T(8,128)(2,1)} %bitcast.19, s32[1024]{0:T(1024)S(1)} %pad_clamp_fusion), kind=kCustom, calls=%fused_computation.1 | custom fusion | bytes 2099200 | tf_op jit(solution)/shard_map/jit(_take)/gather | solution.py:133
  264.4 1.2 gather.15
  265.6 3.6 %multiply_reduce_fusion = bf16[128,1024]{1,0:T(8,128)(2,1)} fusion(f32[128,4]{1,0:T(8,128)S(1)} %copy.53, bf16[128,4,1024]{2,1,0:T(4,128)(2,1)} %gather.15, pred[128,4]{1,0:T(8,128)(4,1)S(1)} %copy.50), kind=kLoop, calls=%fused_computation.11 | loop fusion | flops 1966080 | bytes 1313280 | tf_op jit(solution)/shard_map/reduce_sum | solution.py:135
  (70 shorter events, 2.9 us)
Async XLA Ops:
  7.2 141.6 %copy-start = (bf16[1,256,4096]{2,1,0:T(8,128)(2,1)S(1)}, bf16[1,256,4096]{2,1,0:T(8,128)(2,1)}, u32[]{:S(2)}) copy-start(bf16[1,256,4096]{2,1,0:T(8,128)(2,1)} %param.23) | copy-start | bytes 6291460
  7.2 3.0 %copy-start.2 = (bf16[128,4096]{1,0:T(8,128)(2,1)S(1)}, bf16[128,4096]{1,0:T(8,128)(2,1)}, u32[]{:S(2)}) copy-start(bf16[128,4096]{1,0:T(8,128)(2,1)} %param.17) | copy-start | bytes 3145732
  7.2 210.4 %reduce-scatter.5.cloned.1.call-start = ((), (), s32[]{:S(2)}) async-start(), calls=%async_computation.6 | async-start | bytes 7864320 | tf_op jit(solution)/shard_map/reduce_scatter | solution.py:123
  7.2 3.2 %copy-start.8 = (s32[128,4]{0,1:T(4,128)S(1)}, s32[128,4]{0,1:T(4,128)}, u32[]{:S(2)}) copy-start(s32[128,4]{0,1:T(4,128)} %param.19) | copy-start | bytes 6148
  70.9 76.1 %copy-start.4 = (bf16[1,4096,256]{2,1,0:T(8,128)(2,1)S(1)}, bf16[1,4096,256]{2,1,0:T(8,128)(2,1)}, u32[]{:S(2)}) copy-start(bf16[1,4096,256]{2,1,0:T(8,128)(2,1)} %param.21) | copy-start | bytes 6291460
  144.3 2.7 copy-start.1
  161.4 0.8 copy-start.5
  161.4 4.2 %copy-start.6 = (bf16[256,128]{1,0:T(8,128)(2,1)S(1)}, bf16[256,128]{1,0:T(8,128)(2,1)}, u32[]{:S(2)}) copy-start(bf16[256,128]{1,0:T(8,128)(2,1)} %param.14) | copy-start | bytes 196612
  161.5 8.1 %copy-start.7 = (bf16[256,512]{1,0:T(8,128)(2,1)S(1)}, bf16[256,512]{1,0:T(8,128)(2,1)}, u32[]{:S(2)}) copy-start(bf16[256,512]{1,0:T(8,128)(2,1)} %param.12) | copy-start | bytes 786436
  161.5 8.4 %copy-start.10 = (f32[8]{0:T(128)S(1)}, f32[8]{0:T(128)}, u32[]{:S(2)}) copy-start(f32[8]{0:T(128)} %param.15) | copy-start | bytes 100
  161.5 107.8 %reduce-scatter.3.cloned.1.call-start = ((), (), s32[]{:S(2)}) async-start(), calls=%async_computation.5 | async-start | bytes 2621440 | tf_op jit(solution)/shard_map/reduce_scatter | solution.py:83
  162.3 7.8 %collective-permute-start.1 = (bf16[128,128]{1,0:T(8,128)(2,1)S(1)}, bf16[128,128]{1,0:T(8,128)(2,1)S(1)}, u32[]{:S(2)}, u32[]{:S(2)}) collective-permute-start(bf16[128,128]{1,0:T(8,128)(2,1)S(1)} %slice.20), channel_id=1, source_target_pairs={{0,4},{4,8},{8,12},{12,16},{16,20},{20,24},{24,28},{1,5},{5,9},{9,... | collective-permute-start | bytes 98312 | tf_op jit(solution)/shard_map/ppermute | solution.py:18
  165.6 4.7 %collective-permute-start = (bf16[128,128]{1,0:T(8,128)(2,1)S(1)}, bf16[128,128]{1,0:T(8,128)(2,1)S(1)}, u32[]{:S(2)}, u32[]{:S(2)}) collective-permute-start(bf16[128,128]{1,0:T(8,128)(2,1)S(1)} %slice.18), channel_id=1, source_target_pairs={{0,4},{4,8},{8,12},{12,16},{16,20},{20,24},{24,28},{1,5},{5,9},{9,... | collective-permute-start | bytes 98312 | tf_op jit(solution)/shard_map/ppermute | solution.py:18
  171.6 2.4 copy-start.3
  176.7 46.8 %copy-start.9 = (f32[128,4]{0,1:T(4,128)S(1)}, f32[128,4]{0,1:T(4,128)}, u32[]{:S(2)}) copy-start(f32[128,4]{0,1:T(4,128)} %param.20) | copy-start | bytes 6148
  217.6 42.4 %all-to-all-start.2 = ((bf16[8,96,1024]{2,1,0:T(8,128)(2,1)}), bf16[8,96,1024]{2,1,0:T(8,128)(2,1)}, u32[]{:S(2)}, u32[]{:S(2)}) async-start(bf16[8,96,1024]{2,1,0:T(8,128)(2,1)} %bitcast.68), calls=%async_computation.4 | async-start | bytes 3145728 | tf_op jit(solution)/shard_map/all_to_all | solution.py:126
Sparse Core Ops, SparseCore 0:
  161.6 55.9 reduce-scatter.4
  220.7 31.1 reduce-scatter.2
